TPU v7x, 32 devices: a whole 2x2x4 slice. The times are simulated.
32 devices in a mesh: ep: 8 (over z, y), tp: 4 (over x, core).
Axes of the slice: x: 2, y: 2, z: 4, core: 2. Of those that a mesh axis runs over, the one named last changes fastest.
Arguments:
- conv_value: bfloat16 [4096, 2048], P('ep', 'tp'), may hold values from -6 to 6
- conv_gate: bfloat16 [4096, 2048], P('ep', 'tp'), may hold values from -9 to 9
- conv_kernel: float32 [31, 2048], P(None, 'tp'), may hold values from -20 to 20
- norm_gain: float32 [2048], P('tp'), may hold values from 0.1 to 1.9
- mixer_proj: bfloat16 [2048, 2048], P('tp'), may hold values from -0.125 to 0.125
- moe_in: bfloat16 [4096, 2048], P('ep'), may hold values from -6 to 6
- route_ids: int32 [4096, 2], P('ep'), may hold values from 0 to 7, all different within a row; in each aligned block of 128 rows (0 to 127, 128 to 255, ...) at most 64 rows name the same one
- route_logits: float32 [4096, 2], P('ep'), may hold values from -6 to 6
- moe_gain: float32 [2048], replicated, may hold values from 0.1 to 1.9
- expert_gate: bfloat16 [8, 2048, 2048], P('ep', None, 'tp'), may hold values from -0.26367188 to 0.26367188
- expert_lin: bfloat16 [8, 2048, 2048], P('ep', None, 'tp'), may hold values from -0.26367188 to 0.26367188
- expert_down: bfloat16 [8, 2048, 2048], P('ep', 'tp'), may hold values from -0.052978516 to 0.052978516
Outputs:
- mixer_out: bfloat16 [4096, 2048], P(('ep', 'tp'))
- moe_out: bfloat16 [4096, 2048], P(('ep', 'tp'))
Inputs may be any that keep to these rules, and one draw needn't show every extreme that they name: `route_ids`: every row names 2 different experts. In each aligned block of 128 rows (one device's output rows) no expert is named by more than 64 rows, and in every draw some expert is named by exactly 64 rows of some block.
All inputs are finite; a program needn't handle non-finite values.
Results may differ from a plain program's by a relative error of at most 0.01.
Values may be sent and summed in bfloat16 or wider, within the bound.
A program may use at most 128 MiB of HBM per device.

v0:
```python
import jax
import jax.numpy as jnp
from jax import lax
from jax.experimental import pallas as pl
from jax.experimental.pallas import tpu as pltpu
from jax.sharding import PartitionSpec as P

EPS = 1e-05
LIMIT = 7.0
SLOPE = 1.702
F32 = jnp.float32
BF16 = jnp.bfloat16


def passed_along(block, axis, distance):
    devices = range(lax.axis_size(axis))
    route = [(i - distance, i) for i in devices if i - distance in devices]
    return lax.ppermute(block, axis, route)


def slot_targets(routes, experts, capacity):
    flat = routes.reshape(-1)
    onehot = (flat[:, None] == jnp.arange(experts, dtype=jnp.int32)[None, :]).astype(jnp.int32)
    rank = jnp.sum(jnp.cumsum(onehot, axis=0) * onehot, axis=1) - 1
    return flat * capacity + rank


def remote(src, dst, send, recv, device):
    return pltpu.make_async_remote_copy(
        src_ref=src,
        dst_ref=dst,
        send_sem=send,
        recv_sem=recv,
        device_id=device,
        device_id_type=pl.DeviceIdType.MESH,
    )


def joined(block):
    groups, rows, width = block.shape
    if rows % 16:
        return block.astype(F32).reshape(groups * rows, width).astype(BF16)
    return block.reshape(groups * rows, width)


def layer_kernel(
    packed, act, wmat, gate_hbm, lin_hbm, down_hbm, proj_hbm,
    mix_out, moe_out,
    gate_w, lin_w, down_w, proj_w,
    arrived, part, a_recv, b_send, b_recv, c_send, c_recv,
    m_part, m_a, m_bs, m_b,
    load_sem, sems, m_sems,
):
    experts, cap, width = packed.shape
    rows = moe_out.shape[0]
    ep, tp = lax.axis_index("ep"), lax.axis_index("tp")
    core, side = lax.rem(tp, 2), lax.div(tp, 2)
    xpeer, cpeer = {"tp": lax.rem(tp + 2, 4)}, {"tp": tp + 1 - 2 * core}
    pos, posx = core * 2 + side, core * 2 + 1 - side
    posc, posd = (1 - core) * 2 + side, (1 - core) * 2 + 1 - side

    def chunk(d):
        return lax.rem(ep - d + experts, experts)

    def prim(d):
        e = lax.rem(ep + d, experts)
        return remote(packed.at[e], arrived.at[ep, pos], sems.at[0, d], sems.at[1, d], {"ep": e})

    def prim_in(d):
        slot = arrived.at[chunk(d), pos]
        return remote(slot, slot, sems.at[0, d], sems.at[1, d], {"ep": chunk(d)})

    own = pltpu.make_async_copy(packed.at[ep], arrived.at[ep, pos], load_sem.at[4])

    def hop(d, place, k, peer):
        slot = arrived.at[chunk(d), place]
        return remote(slot, slot, sems.at[k, d], sems.at[k + 1, d], peer)

    def xf(d):
        return hop(d, pos, 2, xpeer)

    def xf_in(d):
        return hop(d, posx, 2, xpeer)

    def cf(d):
        return hop(d, pos, 4, cpeer)

    def cf_in(d):
        return hop(d, posc, 4, cpeer)

    def cf2(d):
        return hop(d, posx, 6, cpeer)

    def cf2_in(d):
        return hop(d, posd, 6, cpeer)

    def give_a(d):
        s = chunk(d)
        return remote(part.at[s, 1 - core], a_recv.at[s], sems.at[8, d], sems.at[9, d], cpeer)

    def give_b(d):
        s = chunk(d)
        return remote(b_send.at[s], b_recv.at[s], sems.at[10, d], sems.at[11, d], xpeer)

    def give_c(d):
        s = chunk(d)
        return remote(c_send.at[s], c_recv.at[ep], sems.at[12, d], sems.at[13, d], {"ep": s})

    def give_c_in(d):
        e = lax.rem(ep + d, experts)
        return remote(c_recv.at[e], c_recv.at[e], sems.at[12, d], sems.at[13, d], {"ep": e})

    mix_a = remote(m_part.at[1 - core], m_a, m_sems.at[0], m_sems.at[1], cpeer)
    mix_b = remote(m_bs, m_b, m_sems.at[2], m_sems.at[3], xpeer)

    own.start()

    @pl.loop(1, experts)
    def _(d):
        prim(d).start()

    loads = [
        pltpu.make_async_copy(proj_hbm, proj_w, load_sem.at[3]),
        pltpu.make_async_copy(gate_hbm, gate_w, load_sem.at[0]),
        pltpu.make_async_copy(lin_hbm, lin_w, load_sem.at[1]),
        pltpu.make_async_copy(down_hbm, down_w, load_sem.at[2]),
    ]
    for load in loads:
        load.start()
    own.wait()
    xf(0).start()
    cf(0).start()

    loads[0].wait()
    for t in range(4):
        m_part[t % 2, t // 2] = jnp.dot(
            act[t * rows : (t + 1) * rows, :], proj_w[...], preferred_element_type=F32
        ).astype(BF16)
    mix_a.start()
    for load in loads[1:]:
        load.wait()

    def ffn(d):
        s = chunk(d)
        x = joined(arrived[s])
        gate = jnp.minimum(jnp.dot(x, gate_w[...], preferred_element_type=F32), LIMIT)
        lin = jnp.clip(jnp.dot(x, lin_w[...], preferred_element_type=F32), -LIMIT, LIMIT)
        hidden = (gate * jax.nn.sigmoid(SLOPE * gate) * (lin + 1.0)).astype(BF16)
        tile = min(512, width)
        for n in range(0, width, tile):
            y = jnp.dot(hidden, down_w[:, n : n + tile], preferred_element_type=F32)
            part[s, :, :, :, n : n + tile] = y.reshape(2, 2, cap, tile).astype(BF16)

    def at_step(i, lag, first=0):
        return jnp.logical_and(i - lag >= first, i - lag < experts)

    @pl.loop(0, experts + 4)
    def _(i):
        @pl.when(at_step(i, 0, 1))
        def _():
            prim_in(i).wait_recv()
            xf(i).start()
            cf(i).start()

        @pl.when(at_step(i, 1))
        def _():
            xf_in(i - 1).wait_recv()
            cf2(i - 1).start()

        @pl.when(at_step(i, 2))
        def _():
            cf_in(i - 2).wait_recv()
            cf2_in(i - 2).wait_recv()
            ffn(i - 2)
            give_a(i - 2).start()

        @pl.when(at_step(i, 3))
        def _():
            d = i - 3
            s = chunk(d)
            give_a(d).wait_recv()
            b_send[s] = (part[s, core, 1 - side].astype(F32) + a_recv[s, 1 - side].astype(F32)).astype(BF16)
            give_b(d).start()

        @pl.when(i == 3)
        def _():
            mix_a.wait_recv()
            m_bs[...] = (m_part[core, 1 - side].astype(F32) + m_a[1 - side].astype(F32)).astype(BF16)
            mix_b.start()

        @pl.when(at_step(i, 4))
        def _():
            d = i - 4
            s = chunk(d)
            give_b(d).wait_recv()
            total = part[s, core, side].astype(F32) + a_recv[s, side].astype(F32) + b_recv[s].astype(F32)

            @pl.when(d == 0)
            def _():
                c_recv[s] = total.astype(BF16)

            @pl.when(d > 0)
            def _():
                c_send[s] = total.astype(BF16)
                give_c(d).start()

    mix_b.wait_recv()
    mix_out[...] = (
        m_part[core, side].astype(F32) + m_a[side].astype(F32) + m_b[...].astype(F32)
    ).astype(BF16)

    @pl.loop(1, experts)
    def _(d):
        give_c_in(d).wait_recv()

    weight = wmat[...]
    high = weight.astype(BF16)
    low = (weight - high.astype(F32)).astype(BF16)
    tile = min(512, width)
    for n in range(0, width, tile):
        results = joined(c_recv[:, :, n : n + tile])
        moe_out[:, n : n + tile] = (
            jnp.dot(high, results, preferred_element_type=F32)
            + jnp.dot(low, results, preferred_element_type=F32)
        ).astype(BF16)

    mix_a.wait_send()
    mix_b.wait_send()

    @pl.loop(0, experts)
    def _(d):
        @pl.when(d > 0)
        def _():
            prim(d).wait_send()
            give_c(d).wait_send()

        xf(d).wait_send()
        cf(d).wait_send()
        cf2(d).wait_send()
        give_a(d).wait_send()
        give_b(d).wait_send()


def shards(
    conv_value,
    conv_gate,
    conv_kernel,
    norm_gain,
    mixer_proj,
    moe_in,
    route_ids,
    route_logits,
    moe_gain,
    expert_gate,
    expert_lin,
    expert_down,
):
    tp_size = lax.axis_size("tp")
    tp_index = lax.axis_index("tp")
    glu = (conv_value.astype(jnp.float32) * jax.nn.sigmoid(conv_gate.astype(jnp.float32))).astype(
        jnp.bfloat16
    )
    reach = conv_kernel.shape[0] - 1
    length = glu.shape[0]
    rim = passed_along(glu[length - reach :], "ep", 1)
    padded = jnp.concatenate([rim, glu], axis=0).astype(jnp.float32)
    conv = jnp.zeros(glu.shape, jnp.float32)
    for tap in range(reach + 1):
        conv = conv + conv_kernel[tap][None, :] * padded[tap : tap + length]
    total, square = lax.psum((jnp.sum(conv, axis=1), jnp.sum(conv * conv, axis=1)), "tp")
    channels = conv.shape[1] * tp_size
    mean = (total / channels)[:, None]
    var = (square / channels)[:, None] - mean * mean
    conv_act = jax.nn.silu((conv - mean) * lax.rsqrt(var + EPS) * norm_gain).astype(jnp.bfloat16)

    rows = moe_in.shape[0] // tp_size
    topk = route_ids.shape[1]
    experts = lax.axis_size("ep")
    capacity = max(2, 2 * rows * topk // experts)
    width = moe_in.shape[1]
    start = tp_index * rows
    block = lax.dynamic_slice_in_dim(moe_in, start, rows, 0).astype(jnp.float32)
    mu = jnp.mean(block, axis=1, keepdims=True)
    va = jnp.mean(jnp.square(block - mu), axis=1, keepdims=True)
    normed = ((block - mu) * lax.rsqrt(va + EPS) * moe_gain).astype(jnp.bfloat16)
    routes = lax.dynamic_slice_in_dim(route_ids, start, rows, 0)
    target = slot_targets(routes, experts, capacity).reshape(rows, topk)
    logits = lax.dynamic_slice_in_dim(route_logits, start, rows, 0)
    expo = jnp.exp(logits)
    weight = expo / jnp.sum(expo, axis=1, keepdims=True)
    slots = jnp.arange(experts * capacity, dtype=jnp.int32)
    hits = target[:, :, None] == slots[None, None, :]
    placed = jnp.any(hits, axis=1).astype(jnp.bfloat16)
    wmat = jnp.sum(jnp.where(hits, weight[:, :, None], 0.0), axis=1)
    packed = lax.dot_general(
        placed, normed, (((0,), (0,)), ((), ())), preferred_element_type=jnp.float32
    ).astype(jnp.bfloat16)
    packed = packed.reshape(experts, capacity, width)

    hid = expert_gate.shape[2]
    chans = conv_act.shape[1]
    vmem = pl.BlockSpec(memory_space=pltpu.VMEM)
    hbm = pl.BlockSpec(memory_space=pl.ANY)
    out = jax.ShapeDtypeStruct((rows, width), BF16)
    mixer_out, moe_out = pl.pallas_call(
        layer_kernel,
        out_shape=(out, out),
        in_specs=[vmem, vmem, vmem, hbm, hbm, hbm, hbm],
        out_specs=(vmem, vmem),
        scratch_shapes=[
            pltpu.VMEM((width, hid), BF16),
            pltpu.VMEM((width, hid), BF16),
            pltpu.VMEM((hid, width), BF16),
            pltpu.VMEM((chans, width), BF16),
            pltpu.VMEM((experts, tp_size, capacity, width), BF16),
            pltpu.VMEM((experts, 2, 2, capacity, width), BF16),
            pltpu.VMEM((experts, 2, capacity, width), BF16),
            pltpu.VMEM((experts, capacity, width), BF16),
            pltpu.VMEM((experts, capacity, width), BF16),
            pltpu.VMEM((experts, capacity, width), BF16),
            pltpu.VMEM((experts, capacity, width), BF16),
            pltpu.VMEM((2, 2, rows, width), BF16),
            pltpu.VMEM((2, rows, width), BF16),
            pltpu.VMEM((rows, width), BF16),
            pltpu.VMEM((rows, width), BF16),
            pltpu.SemaphoreType.DMA((5,)),
            pltpu.SemaphoreType.DMA((14, experts)),
            pltpu.SemaphoreType.DMA((4,)),
        ],
        compiler_params=pltpu.CompilerParams(
            has_side_effects=True, vmem_limit_bytes=60 * 1024 * 1024
        ),
    )(packed, conv_act, wmat, expert_gate[0], expert_lin[0], expert_down[0], mixer_proj)
    return (mixer_out, moe_out)


def solution(mesh):
    placed = (
        P("ep", "tp"),
        P("ep", "tp"),
        P(None, "tp"),
        P("tp"),
        P("tp", None),
        P("ep", None),
        P("ep", None),
        P("ep", None),
        P(),
        P("ep", None, "tp"),
        P("ep", None, "tp"),
        P("ep", "tp", None),
    )
    return jax.shard_map(
        shards,
        mesh=mesh,
        in_specs=placed,
        out_specs=(P(("ep", "tp"), None), P(("ep", "tp"), None)),
        check_vma=False,
    )
```

profile of v0, /device:TPU:0, one launch (start us, length us, event | category | flops | bytes accessed | tf_op | source)
XLA Modules:
  0.0 179.3 jit_solution(3048502723861360594)
XLA Ops:
  0.6 0.0 copy-start
  0.6 0.0 copy-start.1
  0.7 0.0 copy-start.2
  0.7 1.6 multiply_convert_fusion.1
  2.3 4.9 %collective-permute-start = (bf16[30,512]{1,0:T(8,128)(2,1)S(1)}, bf16[30,512]{1,0:T(8,128)(2,1)S(1)}, u32[]{:S(2)}, u32[]{:S(2)}) collective-permute-start(bf16[30,512]{1,0:T(8,128)(2,1)S(1)} %slice.261), channel_id=1, source_target_pairs={{0,4},{4,8},{8,12},{12,16},{16,20},{20,24},{24,28},{1,5},{5,9},{9,... | collective-permute-start | bytes 92168 | tf_op jit(solution)/shard_map/ppermute | solution.py:18
  7.2 1.0 fusion.48
  8.3 1.2 fusion.47
  9.4 0.0 copy-done
  9.5 0.1 copy.20
  9.6 0.1 eq.42
  9.7 0.1 eq.38
  9.9 0.7 fusion.44
  10.6 0.7 broadcast_divide_fusion
  11.3 1.2 convert_reduce_fusion
  12.5 0.0 copy-done.1
  12.5 0.3 fusion.2
  12.8 0.6 reduce-window.6
  13.4 0.2 slice_reduce_fusion
  13.6 0.1 fusion.41
  13.7 0.1 sub.31
  13.9 0.1 copy.19
  13.9 0.1 fusion.39
  14.1 0.0 copy-done.2
  14.1 2.2 %convolution_convert_fusion = bf16[512,2048]{1,0:T(8,128)(2,1)} fusion(pred[128,512]{1,0:T(8,128)(4,1)S(1)} %fusion.39, f32[2048]{0:T(1024)S(1)} %copy-done.2, f32[128]{0:T(128)S(1)} %add_rsqrt_fusion.1, f32[128]{0:T(128)S(1)} %broadcast_multiply_fusion.1, bf16[512,2048]{1,0:T(8,128)(2,1)S(1)} %copy-done.1, s32[]{:T(128)S(6)} %select_n.9), kind=kOutput, calls=%fused_computation | convolution fusion | flops 270794752 | bytes 2696196 | tf_op jit(solution)/shard_map/dot_general | solution.py:295
  16.3 0.8 select_reduce_fusion.wmat
  17.1 0.0 collective-permute-done
  17.1 0.2 maximum_convert_fusion
  17.3 0.0 copy-start.3
  17.3 5.1 %fusion.45 = (f32[512]{0:T(512)S(1)}, f32[512]{0:T(512)S(1)}, f32[512,512]{1,0:T(8,128)S(1)}) fusion(f32[542,512]{1,0:T(8,128)S(1)} %maximum_convert_fusion, f32[512]{0:T(512)S(1)} %bitcast.56, f32[512]{0:T(512)S(1)} %bitcast.57, f32[512]{0:T(512)S(1)} %bitcast.59, f32[512]{0:T(512)S(1)} %bitcast.60, f32[512]{0:T(512)S(1)} %bitcast.61, f32[512]{0:T(512)S(1)} %bitcast.62, ...), kind=kLoop, calls=%fused_computation.97 | loop fusion | flops 16776192 | bytes 33622016 | tf_op jit(solution)/shard_map/reduce_sum | solution.py:270
  22.4 6.3 %all-reduce = (f32[512]{0:T(512)S(1)}, f32[512]{0:T(512)S(1)}) all-reduce(f32[512]{0:T(512)S(1)} %get-tuple-element.3, f32[512]{0:T(512)S(1)} %get-tuple-element.2), channel_id=1, replica_groups=mesh['ep'=8,'tp'=4] {'tp'}, use_global_device_ids=true, to_apply=%region_9.10 | all-reduce | flops 1024 | bytes 8192 | tf_op jit(solution)/shard_map/psum | solution.py:270
  28.7 0.0 copy-done.3
  28.7 1.2 multiply_convert_fusion.act
  29.9 145.7 %shard_map.131 = (bf16[128,2048]{1,0:T(8,128)(2,1)}, bf16[128,2048]{1,0:T(8,128)(2,1)}) custom-call(bf16[8,64,2048]{2,1,0:T(8,128)(2,1)} %bitcast.42, bf16[512,512]{1,0:T(8,128)(2,1)} %multiply_convert_fusion.act, f32[128,512]{1,0:T(8,128)} %select_reduce_fusion.wmat, bf16[2048,512]{1,0:T(8,128)(2,1)} %bitcast.43, bf16[2048,512]{1,0:T(8,128)(2,1)} %bitcast.44, ...), custom_call_target="tpu_custom_call" | custom-call | tf_op jit(solution)/shard_map/pallas_call | solution.py:305
  175.6 1.9 %copy.23 = bf16[128,2048]{1,0:T(8,128)(2,1)} copy(bf16[128,2048]{1,0:T(8,128)(2,1)} %get-tuple-element.42) | data formatting | bytes 1048576
  177.4 1.9 %copy.24 = bf16[128,2048]{1,0:T(8,128)(2,1)} copy(bf16[128,2048]{1,0:T(8,128)(2,1)} %get-tuple-element.43) | data formatting | bytes 1048576
  (10 shorter events, 0.1 us)
Async XLA Ops:
  0.6 8.8 %copy-start = (s32[512,2]{0,1:T(2,128)S(1)}, s32[512,2]{0,1:T(2,128)}, u32[]{:S(2)}) copy-start(s32[512,2]{0,1:T(2,128)} %param.18) | copy-start | bytes 12292
  0.6 11.8 %copy-start.1 = (bf16[512,2048]{1,0:T(8,128)(2,1)S(1)}, bf16[512,2048]{1,0:T(8,128)(2,1)}, u32[]{:S(2)}) copy-start(bf16[512,2048]{1,0:T(8,128)(2,1)} %param.17) | copy-start | bytes 6291460
  0.7 13.4 %copy-start.2 = (f32[2048]{0:T(1024)S(1)}, f32[2048]{0:T(1024)}, u32[]{:S(2)}) copy-start(f32[2048]{0:T(1024)} %param.20) | copy-start | bytes 24580
  2.3 14.8 %collective-permute-start = (bf16[30,512]{1,0:T(8,128)(2,1)S(1)}, bf16[30,512]{1,0:T(8,128)(2,1)S(1)}, u32[]{:S(2)}, u32[]{:S(2)}) collective-permute-start(bf16[30,512]{1,0:T(8,128)(2,1)S(1)} %slice.261), channel_id=1, source_target_pairs={{0,4},{4,8},{8,12},{12,16},{16,20},{20,24},{24,28},{1,5},{5,9},{9,... | collective-permute-start | bytes 92168 | tf_op jit(solution)/shard_map/ppermute | solution.py:18
  17.3 11.4 %copy-start.3 = (f32[512]{0:T(512)S(1)}, f32[512]{0:T(512)}, u32[]{:S(2)}) copy-start(f32[512]{0:T(512)} %param.15) | copy-start | bytes 6148
where the time goes:
time: 180 us; the launch traced here: 179 us
  Pallas kernels  146 us (81%)
  other arithmetic  12.7 us (7%)
  local copies, waits for them, and re-layouts  6.8 us (4%)
  blocking collectives  6.31 us (4%)
  starting transfers between devices  4.9 us (3%)
  matrix products  2.19 us (1%)
    pallas_call x1, Pallas kernels, shards(): pl.pallas_call(layer_kernel, out_shape=(out, out), in_specs=[vmem, vmem,...  146 us
    psum x1, blocking collectives, shards(): lax.psum((jnp.sum(conv, axis=1), jnp.sum(conv * conv, axis=1)), 'tp')  6.31 us
    reduce_sum x1, other arithmetic, shards(): jnp.sum(conv, axis=1)  5.05 us
    ppermute x1, starting transfers between devices, passed_along(): return lax.ppermute(block, axis, route)  4.9 us
    unnamed x11, local copies, waits for them, and re-layouts  3.9 us
  transfers between devices with their start and end apart: 1, of which 0 were waited for; matrix products, arithmetic and copies ran while one was open for 5% of the time, Pallas kernels for 0%

commit v1 on v0

v1 whole, which is shorter than its diff:
```python
import jax
import jax.numpy as jnp
from jax import lax
from jax.experimental import pallas as pl
from jax.experimental.pallas import tpu as pltpu
from jax.sharding import PartitionSpec as P

EPS = 1e-05
LIMIT = 7.0
SLOPE = 1.702
F32 = jnp.float32
BF16 = jnp.bfloat16
LANES = 128
RIM = 32
NEAR = 4


def remote(src, dst, send, recv, device):
    return pltpu.make_async_remote_copy(
        src_ref=src,
        dst_ref=dst,
        send_sem=send,
        recv_sem=recv,
        device_id=device,
        device_id_type=pl.DeviceIdType.MESH,
    )


def joined(block):
    groups, rows, width = block.shape
    if rows % 16:
        return block.astype(F32).reshape(groups * rows, width).astype(BF16)
    return block.reshape(groups * rows, width)


def layer_kernel(
    ids, logits, kern, ngain, mgain,
    moe_hbm, value_hbm, cgate_hbm, gate_hbm, lin_hbm, down_hbm, proj_hbm,
    mix_out, moe_out,
    gate_w, lin_w, down_w, proj_w,
    xrows, normed, slots, weights, far_pack, near_pack,
    arrived, part, a_recv, b_send, b_recv, c_send, c_recv,
    value, cgate, padded, conv, tot, squ, act, rim_send, rim_recv, stat_send, stat_recv,
    m_part, m_a, m_bs, m_b,
    wmat, load_sem, sems, t_sems, m_sems,
):
    experts, _, cap, width = arrived.shape
    rows = moe_out.shape[0]
    length, chans = value.shape
    taps = kern.shape[0]
    groups = experts // NEAR
    ep, tp = lax.axis_index("ep"), lax.axis_index("tp")
    core, side = lax.rem(tp, 2), lax.div(tp, 2)
    xpeer, cpeer = {"tp": lax.rem(tp + 2, 4)}, {"tp": tp + 1 - 2 * core}
    dpeer = {"tp": lax.rem(tp + 3 - 2 * core, 4)}
    pos, posx = core * 2 + side, core * 2 + 1 - side
    mine = core * 2
    grp = lax.div(ep, NEAR)
    mem = lax.rem(ep, NEAR)
    row, col = lax.div(mem, 2), lax.rem(mem, 2)

    def near(k):
        return grp * NEAR + lax.rem(row + k // 2, 2) * 2 + lax.rem(col + k, 2)

    def far(j):
        other = lax.rem(grp + lax.div(j, NEAR) + 1, groups)
        k = lax.rem(j, NEAR)
        inner = jnp.where(other < grp, 1, 0)
        return other, inner, k

    def far_source(j):
        other, inner, k = far(j)
        return other * NEAR + lax.rem(inner + lax.div(k, 2), 2) * 2 + lax.rem(col + k, 2)

    def far_target(j):
        other, inner, k = far(j)
        return other * NEAR + lax.rem(inner + k, 2) * 2 + lax.rem(col + lax.div(k, 2), 2)

    def near_step(i):
        return jnp.logical_or(jnp.logical_or(i < 2, i == 3), i == experts - 1)

    def source(i):
        k = jnp.where(i < 2, i, jnp.where(i == 3, 2, 3))
        close = grp * NEAR + lax.rem(row + lax.div(k, 2), 2) * 2 + lax.rem(col + k, 2)
        distant = far_source(jnp.where(i < 4, 0, jnp.minimum(i - 3, experts - NEAR - 1)))
        return jnp.where(near_step(i), close, distant)

    loads = [
        pltpu.make_async_copy(moe_hbm.at[pl.ds(tp * rows, rows)], xrows.at[0], load_sem.at[0]),
        pltpu.make_async_copy(
            moe_hbm.at[pl.ds(lax.rem(tp + 2, 4) * rows, rows)], xrows.at[1], load_sem.at[1]
        ),
        pltpu.make_async_copy(value_hbm, value, load_sem.at[2]),
        pltpu.make_async_copy(cgate_hbm, cgate, load_sem.at[3]),
        pltpu.make_async_copy(gate_hbm, gate_w, load_sem.at[4]),
        pltpu.make_async_copy(lin_hbm, lin_w, load_sem.at[5]),
        pltpu.make_async_copy(down_hbm, down_w, load_sem.at[6]),
        pltpu.make_async_copy(proj_hbm, proj_w, load_sem.at[7]),
    ]
    for load in loads:
        load.start()

    barrier = pltpu.get_barrier_semaphore()

    @pl.loop(1, experts)
    def _(d):
        pl.semaphore_signal(
            barrier, inc=1, device_id={"ep": lax.rem(ep + d, experts)},
            device_id_type=pl.DeviceIdType.MESH,
        )

    for peer in (xpeer, cpeer, dpeer):
        pl.semaphore_signal(barrier, inc=1, device_id=peer, device_id_type=pl.DeviceIdType.MESH)

    padded_experts = -(-experts // 8) * 8
    before = (
        lax.broadcasted_iota(jnp.int32, (rows, rows), 0)
        < lax.broadcasted_iota(jnp.int32, (rows, rows), 1)
    ).astype(BF16)
    names = lax.broadcasted_iota(jnp.int32, (padded_experts, rows), 0)
    for b, block in ((0, tp), (1, lax.rem(tp + 2, 4))):
        chosen = ids[block]
        first, second = chosen[0:1] == names, chosen[1:2] == names
        taken = jnp.where(jnp.logical_or(first, second), 1.0, 0.0)
        rank = jnp.dot(taken.astype(BF16), before, preferred_element_type=F32)
        place = jnp.where(taken > 0.0, rank, -1.0)
        for e in range(experts):
            slots[b, e] = place[e : e + 1]
        if b == 0:
            expo = jnp.exp(logits[block])
            total = expo[0:1] + expo[1:2]
            share = jnp.where(first, expo[0:1] / total, 0.0) + jnp.where(
                second, expo[1:2] / total, 0.0
            )
            for e in range(experts):
                weights[e] = share[e : e + 1]

    def selected(b, group):
        order = lax.broadcasted_iota(jnp.int32, (cap, rows), 0).astype(F32)
        picks = [jnp.where(slots[b, group * NEAR + m] == order, 1.0, 0.0) for m in range(NEAR)]
        return jnp.concatenate(picks, axis=0).astype(BF16)

    for b in range(2):
        loads[b].wait()
        for r in range(0, rows, 16):
            block = xrows[b, r : r + 16].astype(F32)
            mu = jnp.mean(block, axis=1, keepdims=True)
            block = block - mu
            va = jnp.mean(jnp.square(block), axis=1, keepdims=True)
            normed[b, r : r + 16] = (block * lax.rsqrt(va + EPS) * mgain[...]).astype(BF16)

    tile = min(512, width)
    for b in range(2):
        pick = selected(b, grp)
        where = side if b == 0 else 1 - side
        for n in range(0, width, tile):
            y = jnp.dot(pick, normed[b, :, n : n + tile], preferred_element_type=F32)
            near_pack[:, where, :, n : n + tile] = y.reshape(NEAR, cap, tile).astype(BF16)

    arrived[ep, pl.ds(mine, 2)] = near_pack[mem]

    def gated(start, count, over):
        glu = value[pl.ds(start, count), over].astype(F32) * jax.nn.sigmoid(
            cgate[pl.ds(start, count), over].astype(F32)
        )
        return glu.astype(BF16)

    loads[2].wait()
    loads[3].wait()
    rim_send[...] = gated(length - RIM, RIM, slice(None))
    pl.semaphore_wait(barrier, experts + 2)

    def send_near(k):
        e = near(k)
        return remote(
            near_pack.at[lax.rem(e, NEAR)], arrived.at[ep, pl.ds(mine, 2)],
            sems.at[0, e], sems.at[1, ep], {"ep": e},
        )

    def near_in(s):
        slab = arrived.at[s, pl.ds(mine, 2)]
        return remote(slab, slab, sems.at[0, s], sems.at[1, s], {"ep": s})

    def send_far(j):
        e = far_target(j)
        return remote(
            far_pack.at[e], arrived.at[ep, pos], sems.at[0, e], sems.at[1, ep], {"ep": e}
        )

    def far_in(s):
        slot = arrived.at[s, pos]
        return remote(slot, slot, sems.at[0, s], sems.at[1, s], {"ep": s})

    def xf(s):
        slot = arrived.at[s, pos]
        return remote(slot, slot, sems.at[2, s], sems.at[3, s], xpeer)

    def xf_in(s):
        slot = arrived.at[s, posx]
        return remote(slot, slot, sems.at[2, s], sems.at[3, s], xpeer)

    def cf(s):
        slab = arrived.at[s, pl.ds(mine, 2)]
        return remote(slab, slab, sems.at[4, s], sems.at[5, s], cpeer)

    def cf_in(s):
        slab = arrived.at[s, pl.ds(2 - mine, 2)]
        return remote(slab, slab, sems.at[4, s], sems.at[5, s], cpeer)

    def give_a(s):
        return remote(part.at[s, 1 - core], a_recv.at[s], sems.at[6, s], sems.at[7, s], cpeer)

    def give_b(s):
        return remote(b_send.at[s], b_recv.at[s], sems.at[8, s], sems.at[9, s], xpeer)

    def give_c(s):
        return remote(c_send.at[s], c_recv.at[ep], sems.at[10, s], sems.at[11, ep], {"ep": s})

    def give_c_in(e):
        return remote(c_recv.at[e], c_recv.at[e], sems.at[10, e], sems.at[11, e], {"ep": e})

    after = lax.rem(ep + 1, experts)
    prior = lax.rem(ep + experts - 1, experts)
    rim_out = remote(rim_send, rim_recv, t_sems.at[0, 0], t_sems.at[1, 0], {"ep": after})
    rim_in = remote(rim_recv, rim_recv, t_sems.at[0, 0], t_sems.at[1, 0], {"ep": prior})
    stat_out = [
        remote(stat_send, stat_recv.at[p], t_sems.at[0, p + 1], t_sems.at[1, p + 1], peer)
        for p, peer in enumerate((xpeer, cpeer, dpeer))
    ]
    mix_a = remote(m_part.at[1 - core], m_a, m_sems.at[0], m_sems.at[1], cpeer)
    mix_b = remote(m_bs, m_b, m_sems.at[2], m_sems.at[3], xpeer)

    rim_out.start()
    for k in range(1, NEAR):
        send_near(k).start()
    cf(ep).start()

    @pl.loop(1, groups)
    def _(q):
        other = lax.rem(grp + q, groups)
        pick = selected(0, other)
        for n in range(0, width, tile):
            y = jnp.dot(pick, normed[0, :, n : n + tile], preferred_element_type=F32)
            far_pack[pl.ds(other * NEAR, NEAR), :, n : n + tile] = y.reshape(
                NEAR, cap, tile
            ).astype(BF16)
        for k in range(NEAR):
            send_far((q - 1) * NEAR + k).start()

    strips = chans // LANES

    @pl.loop(0, length // 64)
    def _(r):
        here = pl.multiple_of(r * 64, 64)
        for lane in range(strips):
            at = slice(lane * LANES, (lane + 1) * LANES)
            padded[lane, pl.ds(here + RIM, 64)] = gated(here, 64, at).astype(F32)

    def ffn(s):
        x = joined(arrived[s])
        gate = jnp.minimum(jnp.dot(x, gate_w[...], preferred_element_type=F32), LIMIT)
        lin = jnp.clip(jnp.dot(x, lin_w[...], preferred_element_type=F32), -LIMIT, LIMIT)
        hidden = (gate * jax.nn.sigmoid(SLOPE * gate) * (lin + 1.0)).astype(BF16)
        for n in range(0, width, tile):
            y = jnp.dot(hidden, down_w[:, n : n + tile], preferred_element_type=F32)
            part[s, :, :, :, n : n + tile] = y.reshape(2, 2, cap, tile).astype(BF16)

    def convolve():
        rim_in.wait_recv()
        open_rim = jnp.where(ep > 0, 1.0, 0.0)
        for lane in range(strips):
            padded[lane, 0:RIM] = (
                rim_recv[:, lane * LANES : (lane + 1) * LANES].astype(F32) * open_rim
            )

        @pl.loop(0, length // 64)
        def _(r):
            here = pl.multiple_of(r * 64, 64)
            sums = jnp.zeros((64, LANES), F32)
            squares = jnp.zeros((64, LANES), F32)
            for lane in range(strips):
                value_sum = jnp.zeros((64, LANES), F32)
                for tap in range(taps):
                    value_sum = value_sum + (
                        kern[tap : tap + 1, lane * LANES : (lane + 1) * LANES]
                        * padded[lane, pl.ds(here + (RIM - taps + 1 + tap), 64)]
                    )
                conv[lane, pl.ds(here, 64)] = value_sum
                sums = sums + value_sum
                squares = squares + value_sum * value_sum
            tot[pl.ds(here, 64)] = sums
            squ[pl.ds(here, 64)] = squares

        blocks = length // rows
        for t in range(blocks):
            at = slice(t * rows, (t + 1) * rows)
            stat_send[t : t + 1] = jnp.sum(tot[at].T, axis=0, keepdims=True)
            stat_send[blocks + t : blocks + t + 1] = jnp.sum(squ[at].T, axis=0, keepdims=True)
        for copy in stat_out:
            copy.start()

    def mix():
        for copy in stat_out:
            copy.wait_recv()
        stats = stat_send[...] + stat_recv[0] + stat_recv[1] + stat_recv[2]
        blocks = length // rows
        mean = stats[:blocks] / (chans * 4)
        var = stats[blocks:] / (chans * 4) - mean * mean
        scale = lax.rsqrt(var + EPS)
        for t in range(blocks):
            at = slice(t * rows, (t + 1) * rows)
            middle = jnp.broadcast_to(mean[t : t + 1], (LANES, rows)).T
            spread = jnp.broadcast_to(scale[t : t + 1], (LANES, rows)).T
            for lane in range(strips):
                over = slice(lane * LANES, (lane + 1) * LANES)
                centred = (conv[lane, at] - middle) * spread * ngain[:, over]
                act[at, over] = jax.nn.silu(centred).astype(BF16)
        loads[7].wait()
        for n in range(0, width, tile):
            y = jnp.dot(act[...], proj_w[:, n : n + tile], preferred_element_type=F32)
            for t in range(4):
                m_part[t % 2, t // 2, :, n : n + tile] = y[t * rows : (t + 1) * rows].astype(BF16)
        mix_a.start()

    def due(i, late, step):
        at = i - late

        @pl.when(jnp.logical_and(at >= 0, at < experts))
        def _():
            step(source(at))

    def expert_step(s):
        cf_in(s).wait_recv()
        ffn(s)
        give_a(s).start()

    def first_sum(s):
        give_a(s).wait_recv()
        b_send[s] = (part[s, core, 1 - side].astype(F32) + a_recv[s, 1 - side].astype(F32)).astype(BF16)
        give_b(s).start()

    def second_sum(s):
        give_b(s).wait_recv()
        total = part[s, core, side].astype(F32) + a_recv[s, side].astype(F32) + b_recv[s].astype(F32)

        @pl.when(s == ep)
        def _():
            c_recv[s] = total.astype(BF16)

        @pl.when(s != ep)
        def _():
            c_send[s] = total.astype(BF16)
            give_c(s).start()

    for load in loads[4:7]:
        load.wait()

    def arrival(i, s):
        @pl.when(near_step(i))
        def _():
            near_in(s).wait_recv()
            cf(s).start()

        @pl.when(jnp.logical_not(near_step(i)))
        def _():
            xf_in(s).wait_recv()
            cf(s).start()

    @pl.loop(1, experts + 3)
    def _(i):
        due(i, 1, expert_step)
        due(i, 3, second_sum)
        due(i, 1, first_sum)

        @pl.when(i == 1)
        def _():
            convolve()

        @pl.when(i == 2)
        def _():
            mix()

        @pl.when(i == experts)
        def _():
            mix_a.wait_recv()
            m_bs[...] = (m_part[core, 1 - side].astype(F32) + m_a[1 - side].astype(F32)).astype(BF16)
            mix_b.start()

        @pl.when(i <= experts - NEAR)
        def _():
            s = far_source(i - 1)
            far_in(s).wait_recv()
            xf(s).start()

        due(i, 0, lambda s: arrival(i, s))

    mix_b.wait_recv()
    mix_out[...] = (
        m_part[core, side].astype(F32) + m_a[side].astype(F32) + m_b[...].astype(F32)
    ).astype(BF16)

    order = lax.broadcasted_iota(jnp.int32, (cap, rows), 0).astype(F32)
    per = LANES // cap
    for e in range(0, experts, per):
        stacked = jnp.concatenate(
            [jnp.where(slots[0, e + p] == order, weights[e + p], 0.0) for p in range(per)], axis=0
        ).T
        over = slice(e * cap, e * cap + LANES)
        wmat[:, over] = stacked

    @pl.loop(1, experts)
    def _(d):
        give_c_in(lax.rem(ep + d, experts)).wait_recv()

    weight = wmat[...]
    high = weight.astype(BF16)
    low = (weight - high.astype(F32)).astype(BF16)
    for n in range(0, width, tile):
        results = joined(c_recv[:, :, n : n + tile])
        moe_out[:, n : n + tile] = (
            jnp.dot(high, results, preferred_element_type=F32)
            + jnp.dot(low, results, preferred_element_type=F32)
        ).astype(BF16)

    mix_a.wait_send()
    mix_b.wait_send()
    rim_out.wait_send()
    for copy in stat_out:
        copy.wait_send()
    for k in range(1, NEAR):
        send_near(k).wait_send()

    @pl.loop(0, experts - NEAR)
    def _(j):
        send_far(j).wait_send()
        xf(far_source(j)).wait_send()

    @pl.loop(0, experts)
    def _(s):
        @pl.when(s != ep)
        def _():
            give_c(s).wait_send()

        cf(s).wait_send()
        give_a(s).wait_send()
        give_b(s).wait_send()


def shards(
    conv_value,
    conv_gate,
    conv_kernel,
    norm_gain,
    mixer_proj,
    moe_in,
    route_ids,
    route_logits,
    moe_gain,
    expert_gate,
    expert_lin,
    expert_down,
):
    tp_size = lax.axis_size("tp")
    experts = lax.axis_size("ep")
    tokens, width = moe_in.shape
    rows = tokens // tp_size
    topk = route_ids.shape[1]
    capacity = max(2, 2 * rows * topk // experts)
    hid = expert_gate.shape[2]
    length, chans = conv_value.shape
    padded_experts = -(-experts // 8) * 8
    if tp_size != 4 or experts % NEAR or topk != 2 or length != tokens or rows != LANES:
        raise ValueError("unsupported sizes")

    def by_block(table):
        return table.reshape(tp_size, rows, topk).transpose(0, 2, 1)

    vmem = pl.BlockSpec(memory_space=pltpu.VMEM)
    hbm = pl.BlockSpec(memory_space=pl.ANY)
    out = jax.ShapeDtypeStruct((rows, width), BF16)
    slot_rows = (experts, capacity, width)
    mixer_out, moe_out = pl.pallas_call(
        layer_kernel,
        out_shape=(out, out),
        in_specs=[vmem] * 5 + [hbm] * 7,
        out_specs=(vmem, vmem),
        scratch_shapes=[
            pltpu.VMEM((width, hid), BF16),
            pltpu.VMEM((width, hid), BF16),
            pltpu.VMEM((hid, width), BF16),
            pltpu.VMEM((chans, width), BF16),
            pltpu.VMEM((2, rows, width), BF16),
            pltpu.VMEM((2, rows, width), BF16),
            pltpu.VMEM((2, padded_experts, 1, rows), F32),
            pltpu.VMEM((padded_experts, 1, rows), F32),
            pltpu.VMEM(slot_rows, BF16),
            pltpu.VMEM((NEAR, 2, capacity, width), BF16),
            pltpu.VMEM((experts, tp_size, capacity, width), BF16),
            pltpu.VMEM((experts, 2, 2, capacity, width), BF16),
            pltpu.VMEM((experts, 2, capacity, width), BF16),
            pltpu.VMEM(slot_rows, BF16),
            pltpu.VMEM(slot_rows, BF16),
            pltpu.VMEM(slot_rows, BF16),
            pltpu.VMEM(slot_rows, BF16),
            pltpu.VMEM((length, chans), BF16),
            pltpu.VMEM((length, chans), BF16),
            pltpu.VMEM((chans // LANES, length + RIM, LANES), F32),
            pltpu.VMEM((chans // LANES, length, LANES), F32),
            pltpu.VMEM((length, LANES), F32),
            pltpu.VMEM((length, LANES), F32),
            pltpu.VMEM((length, chans), BF16),
            pltpu.VMEM((RIM, chans), BF16),
            pltpu.VMEM((RIM, chans), BF16),
            pltpu.VMEM((8, LANES), F32),
            pltpu.VMEM((3, 8, LANES), F32),
            pltpu.VMEM((2, 2, rows, width), BF16),
            pltpu.VMEM((2, rows, width), BF16),
            pltpu.VMEM((rows, width), BF16),
            pltpu.VMEM((rows, width), BF16),
            pltpu.VMEM((rows, experts * capacity), F32),
            pltpu.SemaphoreType.DMA((8,)),
            pltpu.SemaphoreType.DMA((12, experts)),
            pltpu.SemaphoreType.DMA((2, 4)),
            pltpu.SemaphoreType.DMA((4,)),
        ],
        compiler_params=pltpu.CompilerParams(
            has_side_effects=True, collective_id=0, vmem_limit_bytes=62 * 1024 * 1024
        ),
    )(
        by_block(route_ids), by_block(route_logits), conv_kernel, norm_gain[None], moe_gain[None],
        moe_in, conv_value, conv_gate, expert_gate[0], expert_lin[0], expert_down[0], mixer_proj,
    )
    return (mixer_out, moe_out)


def solution(mesh):
    placed = (
        P("ep", "tp"),
        P("ep", "tp"),
        P(None, "tp"),
        P("tp"),
        P("tp", None),
        P("ep", None),
        P("ep", None),
        P("ep", None),
        P(),
        P("ep", None, "tp"),
        P("ep", None, "tp"),
        P("ep", "tp", None),
    )
    return jax.shard_map(
        shards,
        mesh=mesh,
        in_specs=placed,
        out_specs=(P(("ep", "tp"), None), P(("ep", "tp"), None)),
        check_vma=False,
    )
```

time: 180 us -> 125 us (0.69)
  Pallas kernels: 146 us -> 121 us
  other arithmetic: 12.7 us -> 0 us
  blocking collectives: 6.31 us -> 0 us
  starting transfers between devices: 4.9 us -> 0 us
  local copies, waits for them, and re-layouts: 6.8 us -> 3.76 us
  matrix products: 2.19 us -> 0 us
    pallas_call x1, Pallas kernels: 146 us -> 121 us  [shards(): pl.pallas_call(layer_kernel, out_shape=(out, out), in_specs=[vmem] * 5 +...]
    reduce_sum x6 -> x0, other arithmetic: 8.17 us -> none  [the longest x1 5.05 us: shards(): jnp.sum(conv, axis=1)]
    psum x1 -> x0, blocking collectives: 6.31 us -> none  [shards(): lax.psum((jnp.sum(conv, axis=1), jnp.sum(conv * conv, axis=1)), 'tp')]
    ppermute x1 -> x0, starting transfers between devices: 4.9 us -> none  [passed_along(): return lax.ppermute(block, axis, route)]
    convert_element_type x4 -> x0, other arithmetic: 2.99 us -> none  [the longest x1 1.65 us: shards(): (conv_value.astype(jnp.float32) * jax.nn.sigmoid(conv_gate.astype(jnp.flo...]
    slice x4 -> x0, local copies, waits for them, and re-layouts: 2.4 us -> none  [the longest x2 2.18 us: shards(): conv = conv + conv_kernel[tap][None, :] * padded[tap:tap + length]]
    dot_general x1 -> x0, matrix products: 2.19 us -> none  [shards(): lax.dot_general(placed, normed, (((0,), (0,)), ((), ())), preferred_eleme...]
    unnamed x11 -> x2, local copies, waits for them, and re-layouts: 3.9 us -> 3.76 us
  transfers between devices with their start and end apart: 1 -> 0, of which waited for: 0 -> 0; matrix products, arithmetic and copies ran while one was open for 5% -> 0% of each run, Pallas kernels for 0% -> 0%
where the time goes in v1:
time: 125 us
  Pallas kernels  121 us (97%)
  local copies, waits for them, and re-layouts  3.76 us (3%)
    pallas_call x1, Pallas kernels, shards(): pl.pallas_call(layer_kernel, out_shape=(out, out), in_specs=[vmem] * 5 +...  121 us
    unnamed x2, local copies, waits for them, and re-layouts  3.76 us

profile of v1, /device:TPU:0, one launch (start us, length us, event | category | flops | bytes accessed | tf_op | source)
XLA Modules:
  0.0 125.2 jit_solution(4811148125449948017)
XLA Ops:
  0.6 120.8 %shard_map.131 = (bf16[128,2048]{1,0:T(8,128)(2,1)}, bf16[128,2048]{1,0:T(8,128)(2,1)}) custom-call(s32[4,2,128]{2,1,0:T(2,128)} %bitcast.15, f32[4,2,128]{2,1,0:T(2,128)} %bitcast.16, f32[31,512]{1,0:T(8,128)} %kern.1, f32[1,512]{1,0:T(1,128)} %bitcast.17, f32[1,2048]{1,0:T(1,128)} %bitcast.14, bf16[512,2048]{1,0:T(8,128)(2,1)} %moe_hbm.1, ...), custom_call_target="tpu_custom_call" | custom-call | tf_op jit(solution)/shard_map/pallas_call | solution.py:482
  121.4 1.9 %copy.16 = bf16[128,2048]{1,0:T(8,128)(2,1)} copy(bf16[128,2048]{1,0:T(8,128)(2,1)} %get-tuple-element.4) | data formatting | bytes 1048576
  123.3 1.9 %copy.17 = bf16[128,2048]{1,0:T(8,128)(2,1)} copy(bf16[128,2048]{1,0:T(8,128)(2,1)} %get-tuple-element.5) | data formatting | bytes 1048576

commit v2 on v1

--- a/solution.py
+++ b/solution.py
@@ -38,11 +38,11 @@
     moe_hbm, value_hbm, cgate_hbm, gate_hbm, lin_hbm, down_hbm, proj_hbm,
     mix_out, moe_out,
     gate_w, lin_w, down_w, proj_w,
-    xrows, normed, slots, weights, far_pack, near_pack,
+    xrows, normed, slots, weights, far_pack, near_pack, tokens, table,
     arrived, part, a_recv, b_send, b_recv, c_send, c_recv,
     value, cgate, padded, conv, tot, squ, act, rim_send, rim_recv, stat_send, stat_recv,
     m_part, m_a, m_bs, m_b,
-    wmat, load_sem, sems, t_sems, m_sems,
+    wmat, load_sem, sems, t_sems, m_sems, g_sems,
 ):
     experts, _, cap, width = arrived.shape
     rows = moe_out.shape[0]
@@ -58,31 +58,23 @@
     grp = lax.div(ep, NEAR)
     mem = lax.rem(ep, NEAR)
     row, col = lax.div(mem, 2), lax.rem(mem, 2)
+    mirror = (1 - row) * 2 + col
 
     def near(k):
         return grp * NEAR + lax.rem(row + k // 2, 2) * 2 + lax.rem(col + k, 2)
 
-    def far(j):
+    def far_source(j):
         other = lax.rem(grp + lax.div(j, NEAR) + 1, groups)
         k = lax.rem(j, NEAR)
-        inner = jnp.where(other < grp, 1, 0)
-        return other, inner, k
-
-    def far_source(j):
-        other, inner, k = far(j)
-        return other * NEAR + lax.rem(inner + lax.div(k, 2), 2) * 2 + lax.rem(col + k, 2)
-
-    def far_target(j):
-        other, inner, k = far(j)
-        return other * NEAR + lax.rem(inner + k, 2) * 2 + lax.rem(col + lax.div(k, 2), 2)
+        return other * NEAR + lax.rem(row + 1 + lax.div(k, 2), 2) * 2 + lax.rem(col + k, 2)
 
     def near_step(i):
-        return jnp.logical_or(jnp.logical_or(i < 2, i == 3), i == experts - 1)
+        return jnp.logical_or(i < 3, i == experts - 1)
 
     def source(i):
-        k = jnp.where(i < 2, i, jnp.where(i == 3, 2, 3))
+        k = jnp.minimum(i, 3)
         close = grp * NEAR + lax.rem(row + lax.div(k, 2), 2) * 2 + lax.rem(col + k, 2)
-        distant = far_source(jnp.where(i < 4, 0, jnp.minimum(i - 3, experts - NEAR - 1)))
+        distant = far_source(jnp.clip(i - 3, 0, experts - NEAR - 1))
         return jnp.where(near_step(i), close, distant)
 
     loads = [
@@ -135,9 +127,9 @@
             for e in range(experts):
                 weights[e] = share[e : e + 1]
 
-    def selected(b, group):
+    def selected(places):
         order = lax.broadcasted_iota(jnp.int32, (cap, rows), 0).astype(F32)
-        picks = [jnp.where(slots[b, group * NEAR + m] == order, 1.0, 0.0) for m in range(NEAR)]
+        picks = [jnp.where(place == order, 1.0, 0.0) for place in places]
         return jnp.concatenate(picks, axis=0).astype(BF16)
 
     for b in range(2):
@@ -150,15 +142,6 @@
             normed[b, r : r + 16] = (block * lax.rsqrt(va + EPS) * mgain[...]).astype(BF16)
 
     tile = min(512, width)
-    for b in range(2):
-        pick = selected(b, grp)
-        where = side if b == 0 else 1 - side
-        for n in range(0, width, tile):
-            y = jnp.dot(pick, normed[b, :, n : n + tile], preferred_element_type=F32)
-            near_pack[:, where, :, n : n + tile] = y.reshape(NEAR, cap, tile).astype(BF16)
-
-    arrived[ep, pl.ds(mine, 2)] = near_pack[mem]
-
     def gated(start, count, over):
         glu = value[pl.ds(start, count), over].astype(F32) * jax.nn.sigmoid(
             cgate[pl.ds(start, count), over].astype(F32)
@@ -168,7 +151,6 @@
     loads[2].wait()
     loads[3].wait()
     rim_send[...] = gated(length - RIM, RIM, slice(None))
-    pl.semaphore_wait(barrier, experts + 2)
 
     def send_near(k):
         e = near(k)
@@ -181,11 +163,50 @@
         slab = arrived.at[s, pl.ds(mine, 2)]
         return remote(slab, slab, sems.at[0, s], sems.at[1, s], {"ep": s})
 
-    def send_far(j):
-        e = far_target(j)
+    def send_tokens(q):
+        other = lax.rem(grp + q, groups)
         return remote(
-            far_pack.at[e], arrived.at[ep, pos], sems.at[0, e], sems.at[1, ep], {"ep": e}
-        )
+            normed.at[0], tokens.at[grp], g_sems.at[0, other], g_sems.at[1, grp],
+            {"ep": other * NEAR + mirror},
+        )
+
+    def tokens_in(other):
+        return remote(
+            tokens.at[other], tokens.at[other], g_sems.at[0, other], g_sems.at[1, other], {"ep": other * NEAR + mirror}
+        )
+
+    def send_table(q):
+        other = lax.rem(grp + q, groups)
+        return remote(
+            slots.at[0, pl.ds(other * NEAR, NEAR)], table.at[grp],
+            g_sems.at[2, other], g_sems.at[3, grp], {"ep": other * NEAR + mirror},
+        )
+
+    def table_in(other):
+        return remote(
+            table.at[other], table.at[other], g_sems.at[2, other], g_sems.at[3, other], {"ep": other * NEAR + mirror}
+        )
+
+    def send_relayed(other, k):
+        e = near(k)
+        place = other * NEAR + lax.rem(e, NEAR)
+        return remote(
+            far_pack.at[place], arrived.at[other * NEAR + mirror, pos],
+            sems.at[0, place], sems.at[1, other * NEAR + mirror], {"ep": e},
+        )
+
+    def relay(other):
+        tokens_in(other).wait_recv()
+        table_in(other).wait_recv()
+        pick = selected([table[other, m] for m in range(NEAR)])
+        for n in range(0, width, tile):
+            y = jnp.dot(pick, tokens[other, :, n : n + tile], preferred_element_type=F32)
+            far_pack[pl.ds(other * NEAR, NEAR), :, n : n + tile] = y.reshape(
+                NEAR, cap, tile
+            ).astype(BF16)
+        for k in range(1, NEAR):
+            send_relayed(other, k).start()
+        arrived[other * NEAR + mirror, pos] = far_pack[other * NEAR + mem]
 
     def far_in(s):
         slot = arrived.at[s, pos]
@@ -227,25 +248,39 @@
         remote(stat_send, stat_recv.at[p], t_sems.at[0, p + 1], t_sems.at[1, p + 1], peer)
         for p, peer in enumerate((xpeer, cpeer, dpeer))
     ]
-    mix_a = remote(m_part.at[1 - core], m_a, m_sems.at[0], m_sems.at[1], cpeer)
-    mix_b = remote(m_bs, m_b, m_sems.at[2], m_sems.at[3], xpeer)
-
+    mix_a = remote(m_part.at[1 - core], m_a, m_sems.at[0, 0], m_sems.at[1, 0], cpeer)
+    half = rows // 2
+    mix_b = [
+        remote(
+            m_bs.at[pl.ds(h * half, half)], m_b.at[pl.ds(h * half, half)],
+            m_sems.at[2, h], m_sems.at[3, h], xpeer,
+        )
+        for h in range(2)
+    ]
+
+    pl.semaphore_wait(barrier, experts + 2)
     rim_out.start()
-    for k in range(1, NEAR):
-        send_near(k).start()
-    cf(ep).start()
 
     @pl.loop(1, groups)
     def _(q):
-        other = lax.rem(grp + q, groups)
-        pick = selected(0, other)
+        send_table(q).start()
+
+    for b in range(2):
+        pick = selected([slots[b, grp * NEAR + m] for m in range(NEAR)])
+        where = side if b == 0 else 1 - side
         for n in range(0, width, tile):
-            y = jnp.dot(pick, normed[0, :, n : n + tile], preferred_element_type=F32)
-            far_pack[pl.ds(other * NEAR, NEAR), :, n : n + tile] = y.reshape(
-                NEAR, cap, tile
-            ).astype(BF16)
-        for k in range(NEAR):
-            send_far((q - 1) * NEAR + k).start()
+            y = jnp.dot(pick, normed[b, :, n : n + tile], preferred_element_type=F32)
+            near_pack[:, where, :, n : n + tile] = y.reshape(NEAR, cap, tile).astype(BF16)
+
+    arrived[ep, pl.ds(mine, 2)] = near_pack[mem]
+    send_near(1).start()
+    cf(ep).start()
+
+    @pl.loop(1, groups)
+    def _(q):
+        send_tokens(q).start()
+
+    send_near(2).start()
 
     strips = chans // LANES
 
@@ -352,6 +387,7 @@
             c_send[s] = total.astype(BF16)
             give_c(s).start()
 
+    convolve()
     for load in loads[4:7]:
         load.wait()
 
@@ -366,35 +402,51 @@
             xf_in(s).wait_recv()
             cf(s).start()
 
-    @pl.loop(1, experts + 3)
+    @pl.loop(1, experts + 2)
     def _(i):
-        due(i, 1, expert_step)
-        due(i, 3, second_sum)
-        due(i, 1, first_sum)
-
-        @pl.when(i == 1)
-        def _():
-            convolve()
-
         @pl.when(i == 2)
-        def _():
-            mix()
-
-        @pl.when(i == experts)
         def _():
             mix_a.wait_recv()
             m_bs[...] = (m_part[core, 1 - side].astype(F32) + m_a[1 - side].astype(F32)).astype(BF16)
-            mix_b.start()
-
-        @pl.when(i <= experts - NEAR)
-        def _():
-            s = far_source(i - 1)
-            far_in(s).wait_recv()
+            mix_b[0].start()
+
+        due(i, 1, expert_step)
+        due(i, 1, first_sum)
+
+        @pl.when(i == 1)
+        def _():
+            mix()
+
+        @pl.when(i == 2)
+        def _():
+            @pl.loop(1, groups)
+            def _(q):
+                relay(lax.rem(grp + q, groups))
+
+        @pl.when(jnp.logical_and(i > 1, i < experts - 2))
+        def _():
+            j = i - 2
+            s = far_source(j)
+
+            @pl.when(lax.rem(j, NEAR) > 0)
+            def _():
+                far_in(s).wait_recv()
+
             xf(s).start()
 
+        @pl.when(i == 4)
+        def _():
+            send_near(3).start()
+
+        @pl.when(i == experts)
+        def _():
+            mix_b[1].start()
+
+        due(i, 2, second_sum)
         due(i, 0, lambda s: arrival(i, s))
 
-    mix_b.wait_recv()
+    for copy in mix_b:
+        copy.wait_recv()
     mix_out[...] = (
         m_part[core, side].astype(F32) + m_a[side].astype(F32) + m_b[...].astype(F32)
     ).astype(BF16)
@@ -423,16 +475,23 @@
         ).astype(BF16)
 
     mix_a.wait_send()
-    mix_b.wait_send()
+    for copy in mix_b:
+        copy.wait_send()
     rim_out.wait_send()
     for copy in stat_out:
         copy.wait_send()
     for k in range(1, NEAR):
         send_near(k).wait_send()
 
+    @pl.loop(1, groups)
+    def _(q):
+        send_table(q).wait_send()
+        send_tokens(q).wait_send()
+        for k in range(1, NEAR):
+            send_relayed(lax.rem(grp + q, groups), k).wait_send()
+
     @pl.loop(0, experts - NEAR)
     def _(j):
-        send_far(j).wait_send()
         xf(far_source(j)).wait_send()
 
     @pl.loop(0, experts)
@@ -495,6 +554,8 @@
             pltpu.VMEM((padded_experts, 1, rows), F32),
             pltpu.VMEM(slot_rows, BF16),
             pltpu.VMEM((NEAR, 2, capacity, width), BF16),
+            pltpu.VMEM((experts // NEAR, rows, width), BF16),
+            pltpu.VMEM((experts // NEAR, NEAR, 1, rows), F32),
             pltpu.VMEM((experts, tp_size, capacity, width), BF16),
             pltpu.VMEM((experts, 2, 2, capacity, width), BF16),
             pltpu.VMEM((experts, 2, capacity, width), BF16),
@@ -521,7 +582,8 @@
             pltpu.SemaphoreType.DMA((8,)),
             pltpu.SemaphoreType.DMA((12, experts)),
             pltpu.SemaphoreType.DMA((2, 4)),
-            pltpu.SemaphoreType.DMA((4,)),
+            pltpu.SemaphoreType.DMA((4, 2)),
+            pltpu.SemaphoreType.DMA((4, experts // NEAR)),
         ],
         compiler_params=pltpu.CompilerParams(
             has_side_effects=True, collective_id=0, vmem_limit_bytes=62 * 1024 * 1024

time: 125 us -> 117 us (0.936)
  Pallas kernels: 121 us -> 112 us
    pallas_call x1, Pallas kernels: 121 us -> 112 us  [shards(): pl.pallas_call(layer_kernel, out_shape=(out, out), in_specs=[vmem] * 5 +...]
where the time goes in v2:
time: 117 us
  Pallas kernels  112 us (96%)
  local copies, waits for them, and re-layouts  3.76 us (3%)
    pallas_call x1, Pallas kernels, shards(): pl.pallas_call(layer_kernel, out_shape=(out, out), in_specs=[vmem] * 5 +...  112 us
    unnamed x2, local copies, waits for them, and re-layouts  3.76 us

profile of v2, /device:TPU:0, one launch (start us, length us, event | category | flops | bytes accessed | tf_op | source)
XLA Modules:
  0.0 116.8 jit_solution(16302649749679597616)
XLA Ops:
  0.6 112.4 %shard_map.131 = (bf16[128,2048]{1,0:T(8,128)(2,1)}, bf16[128,2048]{1,0:T(8,128)(2,1)}) custom-call(s32[4,2,128]{2,1,0:T(2,128)} %bitcast.15, f32[4,2,128]{2,1,0:T(2,128)} %bitcast.16, f32[31,512]{1,0:T(8,128)} %kern.1, f32[1,512]{1,0:T(1,128)} %bitcast.17, f32[1,2048]{1,0:T(1,128)} %bitcast.14, bf16[512,2048]{1,0:T(8,128)(2,1)} %moe_hbm.1, ...), custom_call_target="tpu_custom_call" | custom-call | tf_op jit(solution)/shard_map/pallas_call | solution.py:541
  113.0 1.9 %copy.16 = bf16[128,2048]{1,0:T(8,128)(2,1)} copy(bf16[128,2048]{1,0:T(8,128)(2,1)} %get-tuple-element.4) | data formatting | bytes 1048576
  114.9 1.9 %copy.17 = bf16[128,2048]{1,0:T(8,128)(2,1)} copy(bf16[128,2048]{1,0:T(8,128)(2,1)} %get-tuple-element.5) | data formatting | bytes 1048576

commit v3 on v2

--- a/solution.py
+++ b/solution.py
@@ -42,7 +42,7 @@
     arrived, part, a_recv, b_send, b_recv, c_send, c_recv,
     value, cgate, padded, conv, tot, squ, act, rim_send, rim_recv, stat_send, stat_recv,
     m_part, m_a, m_bs, m_b,
-    wmat, load_sem, sems, t_sems, m_sems, g_sems,
+    wmat, summed, load_sem, sems, t_sems, m_sems, g_sems,
 ):
     experts, _, cap, width = arrived.shape
     rows = moe_out.shape[0]
@@ -69,12 +69,12 @@
         return other * NEAR + lax.rem(row + 1 + lax.div(k, 2), 2) * 2 + lax.rem(col + k, 2)
 
     def near_step(i):
-        return jnp.logical_or(i < 3, i == experts - 1)
+        return jnp.logical_or(i < 3, i == experts - 2)
 
     def source(i):
         k = jnp.minimum(i, 3)
         close = grp * NEAR + lax.rem(row + lax.div(k, 2), 2) * 2 + lax.rem(col + k, 2)
-        distant = far_source(jnp.clip(i - 3, 0, experts - NEAR - 1))
+        distant = far_source(jnp.where(i == experts - 1, i - NEAR, jnp.maximum(i - 3, 0)))
         return jnp.where(near_step(i), close, distant)
 
     loads = [
@@ -387,9 +387,22 @@
             c_send[s] = total.astype(BF16)
             give_c(s).start()
 
-    convolve()
     for load in loads[4:7]:
         load.wait()
+
+    def lay_weights():
+        order = lax.broadcasted_iota(jnp.int32, (cap, rows), 0).astype(F32)
+        for group in range(groups):
+            stacked = jnp.concatenate(
+                [
+                    jnp.where(slots[0, e] == order, weights[e], 0.0)
+                    for e in range(group * NEAR, group * NEAR + NEAR)
+                ],
+                axis=0,
+            ).T
+            high = stacked.astype(BF16)
+            wmat[0, group] = high
+            wmat[1, group] = (stacked - high.astype(F32)).astype(BF16)
 
     def arrival(i, s):
         @pl.when(near_step(i))
@@ -411,6 +424,11 @@
             mix_b[0].start()
 
         due(i, 1, expert_step)
+
+        @pl.when(i == 1)
+        def _():
+            convolve()
+
         due(i, 1, first_sum)
 
         @pl.when(i == 1)
@@ -419,6 +437,8 @@
 
         @pl.when(i == 2)
         def _():
+            lay_weights()
+
             @pl.loop(1, groups)
             def _(q):
                 relay(lax.rem(grp + q, groups))
@@ -449,30 +469,32 @@
         copy.wait_recv()
     mix_out[...] = (
         m_part[core, side].astype(F32) + m_a[side].astype(F32) + m_b[...].astype(F32)
-    ).astype(BF16)
-
-    order = lax.broadcasted_iota(jnp.int32, (cap, rows), 0).astype(F32)
-    per = LANES // cap
-    for e in range(0, experts, per):
-        stacked = jnp.concatenate(
-            [jnp.where(slots[0, e + p] == order, weights[e + p], 0.0) for p in range(per)], axis=0
-        ).T
-        over = slice(e * cap, e * cap + LANES)
-        wmat[:, over] = stacked
-
-    @pl.loop(1, experts)
-    def _(d):
-        give_c_in(lax.rem(ep + d, experts)).wait_recv()
-
-    weight = wmat[...]
-    high = weight.astype(BF16)
-    low = (weight - high.astype(F32)).astype(BF16)
+    )
+
+    def weighted(group, n):
+        results = joined(c_recv[pl.ds(group * NEAR, NEAR), :, n : n + tile])
+        return jnp.dot(wmat[0, group], results, preferred_element_type=F32) + jnp.dot(
+            wmat[1, group], results, preferred_element_type=F32
+        )
+
+    for k in range(1, NEAR):
+        give_c_in(near(k)).wait_recv()
     for n in range(0, width, tile):
-        results = joined(c_recv[:, :, n : n + tile])
-        moe_out[:, n : n + tile] = (
-            jnp.dot(high, results, preferred_element_type=F32)
-            + jnp.dot(low, results, preferred_element_type=F32)
-        ).astype(BF16)
+        summed[:, n : n + tile] = weighted(grp, n)
+
+    @pl.loop(1, groups - 1)
+    def _(q):
+        other = lax.rem(grp + q, groups)
+        for m in range(NEAR):
+            give_c_in(other * NEAR + m).wait_recv()
+        for n in range(0, width, tile):
+            summed[:, n : n + tile] += weighted(other, n)
+
+    last = lax.rem(grp + groups - 1, groups)
+    for m in range(NEAR):
+        give_c_in(last * NEAR + m).wait_recv()
+    for n in range(0, width, tile):
+        moe_out[:, n : n + tile] = summed[:, n : n + tile] + weighted(last, n)
 
     mix_a.wait_send()
     for copy in mix_b:
@@ -536,7 +558,7 @@
 
     vmem = pl.BlockSpec(memory_space=pltpu.VMEM)
     hbm = pl.BlockSpec(memory_space=pl.ANY)
-    out = jax.ShapeDtypeStruct((rows, width), BF16)
+    out = jax.ShapeDtypeStruct((rows, width), F32)
     slot_rows = (experts, capacity, width)
     mixer_out, moe_out = pl.pallas_call(
         layer_kernel,
@@ -578,7 +600,8 @@
             pltpu.VMEM((2, rows, width), BF16),
             pltpu.VMEM((rows, width), BF16),
             pltpu.VMEM((rows, width), BF16),
-            pltpu.VMEM((rows, experts * capacity), F32),
+            pltpu.VMEM((2, experts // NEAR, rows, NEAR * capacity), BF16),
+            pltpu.VMEM((rows, width), F32),
             pltpu.SemaphoreType.DMA((8,)),
             pltpu.SemaphoreType.DMA((12, experts)),
             pltpu.SemaphoreType.DMA((2, 4)),
@@ -592,7 +615,7 @@
         by_block(route_ids), by_block(route_logits), conv_kernel, norm_gain[None], moe_gain[None],
         moe_in, conv_value, conv_gate, expert_gate[0], expert_lin[0], expert_down[0], mixer_proj,
     )
-    return (mixer_out, moe_out)
+    return (mixer_out.astype(BF16), moe_out.astype(BF16))
 
 
 def solution(mesh):

time: 117 us -> 112 us (0.957)
  Pallas kernels: 112 us -> 108 us
  local copies, waits for them, and re-layouts: 3.76 us -> 0.01 us
  other arithmetic: 0 us -> 3.03 us
    pallas_call x1, Pallas kernels: 112 us -> 108 us  [shards(): pl.pallas_call(layer_kernel, out_shape=(out, out), in_specs=[vmem] * 5 +...]
    unnamed x2, local copies, waits for them, and re-layouts: 3.76 us -> 0.01 us
    convert_element_type x0 -> x2, other arithmetic: none -> 3.03 us  [shards(): return (mixer_out.astype(BF16), moe_out.astype(BF16))]
where the time goes in v3:
time: 112 us
  Pallas kernels  108 us (96%)
  other arithmetic  3.03 us (3%)
    pallas_call x1, Pallas kernels, shards(): pl.pallas_call(layer_kernel, out_shape=(out, out), in_specs=[vmem] * 5 +...  108 us
    convert_element_type x2, other arithmetic, shards(): return (mixer_out.astype(BF16), moe_out.astype(BF16))  3.03 us

profile of v3, /device:TPU:0, one launch (start us, length us, event | category | flops | bytes accessed | tf_op | source)
XLA Modules:
  0.0 111.6 jit_solution(7591848866748647527)
XLA Ops:
  0.6 107.9 %shard_map.131 = (f32[128,2048]{1,0:T(8,128)}, f32[128,2048]{1,0:T(8,128)}) custom-call(s32[4,2,128]{2,1,0:T(2,128)} %bitcast.15, f32[4,2,128]{2,1,0:T(2,128)} %bitcast.16, f32[31,512]{1,0:T(8,128)} %kern.1, f32[1,512]{1,0:T(1,128)} %bitcast.17, f32[1,2048]{1,0:T(1,128)} %bitcast.14, bf16[512,2048]{1,0:T(8,128)(2,1)} %moe_hbm.1, bf16[512,512]{1,0:T(8,128)(2,1)} %value_hbm.1, ...), custom_call_target="tpu_custom_call" | custom-call | tf_op jit(solution)/shard_map/pallas_call | solution.py:563
  108.5 0.0 copy-start
  108.6 2.2 %convert_element_type.6 = bf16[128,2048]{1,0:T(8,128)(2,1)} convert(f32[128,2048]{1,0:T(8,128)} %get-tuple-element.4) | non-fusion elementwise | flops 262144 | bytes 1572864 | tf_op jit(solution)/shard_map/convert_element_type | solution.py:618
  110.7 0.0 copy-done
  110.7 0.9 convert_element_type.7
Async XLA Ops:
  108.5 2.2 %copy-start = (f32[128,2048]{1,0:T(8,128)S(1)}, f32[128,2048]{1,0:T(8,128)}, u32[]{:S(2)}) copy-start(f32[128,2048]{1,0:T(8,128)} %get-tuple-element.5) | copy-start | bytes 3145732

commit v4 on v3

--- a/solution.py
+++ b/solution.py
@@ -42,7 +42,7 @@
     arrived, part, a_recv, b_send, b_recv, c_send, c_recv,
     value, cgate, padded, conv, tot, squ, act, rim_send, rim_recv, stat_send, stat_recv,
     m_part, m_a, m_bs, m_b,
-    wmat, summed, load_sem, sems, t_sems, m_sems, g_sems,
+    wmat, summed, mix_stage, load_sem, sems, t_sems, m_sems, g_sems,
 ):
     experts, _, cap, width = arrived.shape
     rows = moe_out.shape[0]
@@ -59,6 +59,7 @@
     mem = lax.rem(ep, NEAR)
     row, col = lax.div(mem, 2), lax.rem(mem, 2)
     mirror = (1 - row) * 2 + col
+    outer = row == lax.rem(grp, 2)
 
     def near(k):
         return grp * NEAR + lax.rem(row + k // 2, 2) * 2 + lax.rem(col + k, 2)
@@ -204,7 +205,7 @@
             far_pack[pl.ds(other * NEAR, NEAR), :, n : n + tile] = y.reshape(
                 NEAR, cap, tile
             ).astype(BF16)
-        for k in range(1, NEAR):
+        for k in range(1, NEAR - 1):
             send_relayed(other, k).start()
         arrived[other * NEAR + mirror, pos] = far_pack[other * NEAR + mem]
 
@@ -300,6 +301,27 @@
             y = jnp.dot(hidden, down_w[:, n : n + tile], preferred_element_type=F32)
             part[s, :, :, :, n : n + tile] = y.reshape(2, 2, cap, tile).astype(BF16)
 
+    def conv_rows(r):
+        here = pl.multiple_of(r * 64, 64) if not isinstance(r, int) else r * 64
+        sums = jnp.zeros((64, LANES), F32)
+        squares = jnp.zeros((64, LANES), F32)
+        for lane in range(strips):
+            value_sum = jnp.zeros((64, LANES), F32)
+            for tap in range(taps):
+                value_sum = value_sum + (
+                    kern[tap : tap + 1, lane * LANES : (lane + 1) * LANES]
+                    * padded[lane, pl.ds(here + (RIM - taps + 1 + tap), 64)]
+                )
+            conv[lane, pl.ds(here, 64)] = value_sum
+            sums = sums + value_sum
+            squares = squares + value_sum * value_sum
+        tot[pl.ds(here, 64)] = sums
+        squ[pl.ds(here, 64)] = squares
+
+    @pl.loop(1, length // 64)
+    def _(r):
+        conv_rows(r)
+
     def convolve():
         rim_in.wait_recv()
         open_rim = jnp.where(ep > 0, 1.0, 0.0)
@@ -308,24 +330,7 @@
                 rim_recv[:, lane * LANES : (lane + 1) * LANES].astype(F32) * open_rim
             )
 
-        @pl.loop(0, length // 64)
-        def _(r):
-            here = pl.multiple_of(r * 64, 64)
-            sums = jnp.zeros((64, LANES), F32)
-            squares = jnp.zeros((64, LANES), F32)
-            for lane in range(strips):
-                value_sum = jnp.zeros((64, LANES), F32)
-                for tap in range(taps):
-                    value_sum = value_sum + (
-                        kern[tap : tap + 1, lane * LANES : (lane + 1) * LANES]
-                        * padded[lane, pl.ds(here + (RIM - taps + 1 + tap), 64)]
-                    )
-                conv[lane, pl.ds(here, 64)] = value_sum
-                sums = sums + value_sum
-                squares = squares + value_sum * value_sum
-            tot[pl.ds(here, 64)] = sums
-            squ[pl.ds(here, 64)] = squares
-
+        conv_rows(0)
         blocks = length // rows
         for t in range(blocks):
             at = slice(t * rows, (t + 1) * rows)
@@ -454,6 +459,12 @@
 
             xf(s).start()
 
+        @pl.when(i == jnp.where(outer, 3, 2))
+        def _():
+            @pl.loop(1, groups)
+            def _(q):
+                send_relayed(lax.rem(grp + q, groups), NEAR - 1).start()
+
         @pl.when(i == 4)
         def _():
             send_near(3).start()
@@ -467,9 +478,12 @@
 
     for copy in mix_b:
         copy.wait_recv()
-    mix_out[...] = (
+    mix_stage[...] = (
         m_part[core, side].astype(F32) + m_a[side].astype(F32) + m_b[...].astype(F32)
     )
+
+    mix_store = pltpu.make_async_copy(mix_stage, mix_out, load_sem.at[0])
+    mix_store.start()
 
     def weighted(group, n):
         results = joined(c_recv[pl.ds(group * NEAR, NEAR), :, n : n + tile])
@@ -493,9 +507,20 @@
     last = lax.rem(grp + groups - 1, groups)
     for m in range(NEAR):
         give_c_in(last * NEAR + m).wait_recv()
+    stores = []
     for n in range(0, width, tile):
-        moe_out[:, n : n + tile] = summed[:, n : n + tile] + weighted(last, n)
-
+        over = slice(n, n + tile)
+        summed[:, over] += weighted(last, n)
+        stores.append(
+            pltpu.make_async_copy(
+                summed.at[:, over], moe_out.at[:, over], load_sem.at[1 + n // tile]
+            )
+        )
+        stores[-1].start()
+
+    mix_store.wait()
+    for store in stores:
+        store.wait()
     mix_a.wait_send()
     for copy in mix_b:
         copy.wait_send()
@@ -564,7 +589,7 @@
         layer_kernel,
         out_shape=(out, out),
         in_specs=[vmem] * 5 + [hbm] * 7,
-        out_specs=(vmem, vmem),
+        out_specs=(hbm, hbm),
         scratch_shapes=[
             pltpu.VMEM((width, hid), BF16),
             pltpu.VMEM((width, hid), BF16),
@@ -602,6 +627,7 @@
             pltpu.VMEM((rows, width), BF16),
             pltpu.VMEM((2, experts // NEAR, rows, NEAR * capacity), BF16),
             pltpu.VMEM((rows, width), F32),
+            pltpu.VMEM((rows, width), F32),
             pltpu.SemaphoreType.DMA((8,)),
             pltpu.SemaphoreType.DMA((12, experts)),
             pltpu.SemaphoreType.DMA((2, 4)),

time: 112 us -> 111 us (level)
  no operation moved by 1% of the time
where the time goes in v4:
time: 111 us
  Pallas kernels  107 us (96%)
  other arithmetic  3.03 us (3%)
    pallas_call x1, Pallas kernels, shards(): pl.pallas_call(layer_kernel, out_shape=(out, out), in_specs=[vmem] * 5 +...  107 us
    convert_element_type x2, other arithmetic, shards(): return (mixer_out.astype(BF16), moe_out.astype(BF16))  3.03 us

profile of v4, /device:TPU:0, one launch (start us, length us, event | category | flops | bytes accessed | tf_op | source)
XLA Modules:
  0.0 110.7 jit_solution(4977292878836947253)
XLA Ops:
  0.6 107.0 %shard_map.131 = (f32[128,2048]{1,0:T(8,128)}, f32[128,2048]{1,0:T(8,128)}) custom-call(s32[4,2,128]{2,1,0:T(2,128)} %bitcast.15, f32[4,2,128]{2,1,0:T(2,128)} %bitcast.16, f32[31,512]{1,0:T(8,128)} %kern.1, f32[1,512]{1,0:T(1,128)} %bitcast.17, f32[1,2048]{1,0:T(1,128)} %bitcast.14, bf16[512,2048]{1,0:T(8,128)(2,1)} %moe_hbm.1, bf16[512,512]{1,0:T(8,128)(2,1)} %value_hbm.1, ...), custom_call_target="tpu_custom_call" | custom-call | tf_op jit(solution)/shard_map/pallas_call | solution.py:588
  107.7 0.0 copy-start
  107.7 2.2 %convert_element_type.6 = bf16[128,2048]{1,0:T(8,128)(2,1)} convert(f32[128,2048]{1,0:T(8,128)} %get-tuple-element.4) | non-fusion elementwise | flops 262144 | bytes 1572864 | tf_op jit(solution)/shard_map/convert_element_type | solution.py:644
  109.9 0.0 copy-done
  109.9 0.9 convert_element_type.7
Async XLA Ops:
  107.7 2.2 %copy-start = (f32[128,2048]{1,0:T(8,128)S(1)}, f32[128,2048]{1,0:T(8,128)}, u32[]{:S(2)}) copy-start(f32[128,2048]{1,0:T(8,128)} %get-tuple-element.5) | copy-start | bytes 3145732
